TPU v7x, 32 devices: a whole 2x2x4 slice. The times are simulated.
32 devices in a mesh: sp: 8 (over z, x), tp: 4 (over y, core).
Axes of the slice: x: 2, y: 2, z: 4, core: 2. Of those that a mesh axis runs over, the one named last changes fastest.
Arguments:
- saved_tokens: bfloat16 [1536, 2048], P('sp'), may hold values from -3.75 to 3.75
- cotangent: bfloat16 [1536, 2048], P('sp'), may hold values from -6 to 6
- routes: int32 [1536, 2], P('sp'), may hold values from 0 to 7, all different within a row; in each aligned block of 192 rows (0 to 191, 192 to 383, ...) at most 96 rows name the same one
- route_weights: float32 [1536, 2], P('sp'), may hold values from 0.2 to 1
- gate_in: bfloat16 [1536, 1024], P('sp', 'tp'), may hold values from -6 to 6
- conv_in: bfloat16 [1536, 1024], P('sp', 'tp'), may hold values from -6 to 6
- value_in: bfloat16 [1536, 1024], P('sp', 'tp'), may hold values from -6 to 6
- conv_taps: float32 [3, 1024], replicated, may hold values from -3.5 to 3.5
- out_weight: bfloat16 [2048, 1024], P(None, 'tp'), may hold values from -0.1875 to 0.1875
- gate_proj: bfloat16 [8, 2048, 2048], P('sp', None, 'tp'), may hold values from -0.125 to 0.125
- up_proj: bfloat16 [8, 2048, 2048], P('sp', None, 'tp'), may hold values from -0.125 to 0.125
- down_proj: bfloat16 [8, 2048, 2048], P('sp', 'tp'), may hold values from -0.125 to 0.125
Outputs:
- gate_proj_grad: float32 [8, 2048, 2048], P('sp', None, 'tp')
- up_proj_grad: float32 [8, 2048, 2048], P('sp', None, 'tp')
- down_proj_grad: float32 [8, 2048, 2048], P('sp', 'tp')
- out_weight_grad: float32 [2048, 1024], P('sp', 'tp')
- token_grad: bfloat16 [1536, 2048], P('sp', 'tp')
- gate_in_grad: bfloat16 [1536, 1024], P('sp', 'tp')
- conv_in_grad: bfloat16 [1536, 1024], P('sp', 'tp')
- value_in_grad: bfloat16 [1536, 1024], P('sp', 'tp')
Inputs may be any that keep to these rules, and one draw needn't show every extreme that they name: `routes`: within each aligned block of 192 tokens at most 96 assignments name one expert, a bound that some block reaches of them; the 2 experts of a token differ.
All inputs are finite; a program needn't handle non-finite values.
Results may differ from a plain program's by a relative error of at most 0.0063.
Values may be sent and summed in bfloat16 or wider, within the bound.
A program may use at most 64 MiB of HBM per device.

v0:
```python
import jax
import jax.numpy as jnp
from jax import lax
from jax.sharding import PartitionSpec as P

CLAMP_LIMIT = 7.0
SILU_ALPHA = 1.702


def padded(cells, sides, width):
    for axis, dim in sides:
        count = lax.axis_size(axis)
        ends = count - 1
        head = lax.slice_in_dim(cells, 0, width, axis=dim)
        tail = lax.slice_in_dim(cells, cells.shape[dim] - width, cells.shape[dim], axis=dim)
        cells = jnp.concatenate(
            [
                lax.ppermute(tail, axis, [(i, (i + 1) % count) for i in range(ends)]),
                cells,
                lax.ppermute(head, axis, [((i + 1) % count, i) for i in range(ends)]),
            ],
            axis=dim,
        )
    return cells


def contract_rows(left, right):
    return lax.dot_general(
        left, right, (((0,), (0,)), ((), ())), preferred_element_type=jnp.float32
    )


def contract_cols(left, right):
    return lax.dot_general(
        left, right, (((1,), (1,)), ((), ())), preferred_element_type=jnp.float32
    )


def expert_backward(rows_in, grads_in, w_gate, w_up, w_down):
    gate_pre = jnp.dot(rows_in, w_gate, preferred_element_type=jnp.float32)
    up_pre = jnp.dot(rows_in, w_up, preferred_element_type=jnp.float32)
    gate_clip = jnp.minimum(gate_pre, CLAMP_LIMIT)
    up_clip = jnp.clip(up_pre, -CLAMP_LIMIT, CLAMP_LIMIT)
    sigmoid_gate = jax.nn.sigmoid(SILU_ALPHA * gate_clip)
    gated_act = gate_clip * sigmoid_gate
    hidden = ((up_clip + 1.0) * gated_act).astype(jnp.bfloat16)
    d_hidden = contract_cols(grads_in, w_down)
    d_up = jnp.where(jnp.abs(up_pre) < CLAMP_LIMIT, d_hidden * gated_act, 0.0).astype(jnp.bfloat16)
    gate_slope = sigmoid_gate + SILU_ALPHA * gate_clip * sigmoid_gate * (1.0 - sigmoid_gate)
    d_gate = jnp.where(gate_pre < CLAMP_LIMIT, d_hidden * (up_clip + 1.0) * gate_slope, 0.0).astype(
        jnp.bfloat16
    )
    down_grad = contract_rows(hidden, grads_in)
    gate_grad = contract_rows(rows_in, d_gate)
    up_grad = contract_rows(rows_in, d_up)
    partial_value = contract_cols(d_gate, w_gate) + contract_cols(d_up, w_up)
    return (gate_grad, up_grad, down_grad, partial_value.astype(jnp.bfloat16))


def local(
    saved_tokens,
    cotangent,
    routes,
    route_weights,
    gate_in,
    conv_in,
    value_in,
    conv_taps,
    out_weight,
    gate_proj,
    up_proj,
    down_proj,
):
    tok_rows, model_width = saved_tokens.shape
    top_count = routes.shape[1]
    expert_count = lax.axis_size("sp")
    tp_count = lax.axis_size("tp")
    capacity = 2 * tok_rows * top_count // expert_count
    assigns = tok_rows * top_count
    part_width = model_width // tp_count
    offset = lax.axis_index("tp") * part_width
    flat_routes = routes.reshape(assigns)
    onehot = (flat_routes[:, None] == jnp.arange(expert_count, dtype=jnp.int32)[None, :]).astype(
        jnp.int32
    )
    slot_rank = jnp.sum((jnp.cumsum(onehot, axis=0) - 1) * onehot, axis=1)
    slot_index = flat_routes * capacity + slot_rank
    slot_owner = (
        jnp.full((expert_count * capacity,), assigns, jnp.int32)
        .at[slot_index]
        .set(jnp.arange(assigns, dtype=jnp.int32))
    )
    zero_row = jnp.zeros((1, model_width), jnp.bfloat16)
    token_rows = jnp.concatenate([saved_tokens, zero_row], 0)[slot_owner // top_count]
    scaled = (route_weights[:, :, None] * cotangent.astype(jnp.float32)[:, None, :]).astype(
        jnp.bfloat16
    )
    grad_rows = jnp.concatenate([scaled.reshape(assigns, model_width), zero_row], 0)[slot_owner]
    send_tokens = token_rows.reshape(expert_count, capacity, model_width)
    send_grads = grad_rows.reshape(expert_count, capacity, model_width)
    sliced = (
        lax.dynamic_slice_in_dim(send_tokens, offset, part_width, 2),
        lax.dynamic_slice_in_dim(send_grads, offset, part_width, 2),
    )
    arrived = (
        lax.all_to_all(sliced[0], "sp", split_axis=0, concat_axis=0, tiled=True),
        lax.all_to_all(sliced[1], "sp", split_axis=0, concat_axis=0, tiled=True),
    )
    recv_tokens, recv_grads = (
        lax.all_gather(arrived[0], "tp", axis=2, tiled=True),
        lax.all_gather(arrived[1], "tp", axis=2, tiled=True),
    )
    gate_grad, up_grad, down_grad, partial_value = expert_backward(
        recv_tokens.reshape(-1, model_width),
        recv_grads.reshape(-1, model_width),
        gate_proj[0],
        up_proj[0],
        down_proj[0],
    )
    grouped = partial_value.reshape(expert_count * capacity, tp_count, part_width)
    pieces = lax.all_to_all(grouped, "tp", split_axis=1, concat_axis=1, tiled=True)
    shares = jnp.sum(pieces.astype(jnp.float32), axis=1).reshape(expert_count, capacity, part_width)
    returned = lax.all_to_all(shares, "sp", split_axis=0, concat_axis=0, tiled=True)
    picked = returned.reshape(-1, part_width)[slot_index]
    combined = jnp.sum(picked.reshape(tok_rows, top_count, part_width), axis=1)
    own_cot = lax.dynamic_slice_in_dim(cotangent, offset, part_width, 1).astype(jnp.float32)
    token_grad = (own_cot + combined).astype(jnp.bfloat16)
    residual = lax.all_gather(token_grad, "tp", axis=1, tiled=True)
    channels = gate_in.shape[1]
    d_conv_out = jnp.dot(residual, out_weight, preferred_element_type=jnp.float32)
    gate_f32 = gate_in.astype(jnp.float32)
    conv_f32 = conv_in.astype(jnp.float32)
    value_f32 = value_in.astype(jnp.float32)
    product = conv_f32 * value_f32
    back_signal = d_conv_out * gate_f32
    rimmed = padded(jnp.concatenate([product, back_signal], 1), (("sp", 0),), 1)
    prod_rim = rimmed[:, :channels]
    grad_rim = rimmed[:, channels:]
    my_taps = lax.dynamic_slice_in_dim(conv_taps, lax.axis_index("tp") * channels, channels, 1)
    conv_out = my_taps[0] * prod_rim[:-2] + my_taps[1] * prod_rim[1:-1] + my_taps[2] * prod_rim[2:]
    d_product = my_taps[0] * grad_rim[2:] + my_taps[1] * grad_rim[1:-1] + my_taps[2] * grad_rim[:-2]
    gate_in_grad = (d_conv_out * conv_out).astype(jnp.bfloat16)
    conv_in_grad = (d_product * value_f32).astype(jnp.bfloat16)
    value_in_grad = (d_product * conv_f32).astype(jnp.bfloat16)
    mixed_act = (gate_f32 * conv_out).astype(jnp.bfloat16)
    out_weight_grad = lax.psum_scatter(
        contract_rows(residual, mixed_act), "sp", scatter_dimension=0, tiled=True
    )
    return (
        gate_grad[None],
        up_grad[None],
        down_grad[None],
        out_weight_grad,
        token_grad,
        gate_in_grad,
        conv_in_grad,
        value_in_grad,
    )


def solution(mesh):
    in_specs = (
        P("sp", None),
        P("sp", None),
        P("sp", None),
        P("sp", None),
        P("sp", "tp"),
        P("sp", "tp"),
        P("sp", "tp"),
        P(),
        P(None, "tp"),
        P("sp", None, "tp"),
        P("sp", None, "tp"),
        P("sp", "tp", None),
    )
    out_specs = (
        P("sp", None, "tp"),
        P("sp", None, "tp"),
        P("sp", "tp", None),
        P("sp", "tp"),
        P("sp", "tp"),
        P("sp", "tp"),
        P("sp", "tp"),
        P("sp", "tp"),
    )
    return jax.shard_map(local, mesh=mesh, in_specs=in_specs, out_specs=out_specs, check_vma=False)
```

profile of v0, /device:TPU:0, one launch (start us, length us, event | category | flops | bytes accessed | tf_op | source)
XLA Modules:
  0.0 314.1 jit_solution(3205792691582930578)
XLA Ops:
  10.7 2.9 scatter_custom_fusion
  13.6 1.2 concatenate.18
  14.8 4.2 %gather_fusion = bf16[768,2048]{1,0:T(8,128)(2,1)} fusion(bf16[193,2048]{1,0:T(8,128)(2,1)S(1)} %concatenate.18, s32[1024]{0:T(1024)S(1)} %get-tuple-element.22), kind=kCustom, calls=%fused_computation | custom fusion | bytes 6294528 | tf_op jit(solution)/shard_map/gather | solution.py:94
  19.1 1.3 constant_dynamic-slice_fusion.2
  20.3 27.3 %all_to_all.20 = bf16[8,96,512]{2,1,0:T(8,128)(2,1)} all-to-all(bf16[8,96,512]{2,1,0:T(8,128)(2,1)S(1)} %constant_dynamic-slice_fusion.2), channel_id=1, replica_groups=mesh['sp'=8,'tp'=4] {'sp'}, dimensions={0} | all-to-all | bytes 1572864 | tf_op jit(solution)/shard_map/all_to_all | solution.py:106
  47.7 3.3 %mul.141 = f32[192,2,2048]{2,1,0:T(2,128)} broadcast(bf16[192,2048]{1,0:T(8,128)(2,1)S(1)} %copy-done.3), dimensions={0,2} | broadcast | bytes 3932160 | tf_op jit(solution)/shard_map/mul | solution.py:95
  51.0 5.4 %mul.142 = f32[384,2048]{1,0:T(8,128)} reshape(f32[192,2,2048]{2,1,0:T(2,128)} %mul.141) | data formatting | bytes 6291456 | tf_op jit(solution)/shard_map/mul | solution.py:95
  56.7 2.1 multiply_convert_fusion
  58.8 1.3 concatenate.19
  60.1 8.7 %gather_fusion.1 = bf16[768,2048]{1,0:T(8,128)(2,1)} fusion(bf16[385,2048]{1,0:T(8,128)(2,1)} %concatenate.19, s32[1024]{0:T(1024)S(1)} %get-tuple-element.21), kind=kCustom, calls=%fused_computation.1 | custom fusion | bytes 6294528 | tf_op jit(solution)/shard_map/gather | solution.py:98
  68.8 1.2 constant_dynamic-slice_fusion.1
  70.0 23.4 %all_to_all.21 = bf16[8,96,512]{2,1,0:T(8,128)(2,1)} all-to-all(bf16[8,96,512]{2,1,0:T(8,128)(2,1)S(1)} %constant_dynamic-slice_fusion.1), channel_id=1, replica_groups=mesh['sp'=8,'tp'=4] {'sp'}, dimensions={0} | all-to-all | bytes 1572864 | tf_op jit(solution)/shard_map/all_to_all | solution.py:107
  93.5 5.6 %fusion.1 = f32[768,512]{1,0:T(8,128)} fusion(bf16[768,2048]{1,0:T(8,128)(2,1)} %bitcast.70, bf16[1,2048,512]{2,1,0:T(8,128)(2,1)} %param.22), kind=kOutput, calls=%fused_computation.12 | convolution fusion | flops 1610612736 | bytes 6815744 | tf_op jit(solution)/shard_map/dot_general | solution.py:41
  99.1 3.0 fusion.7
  102.1 19.1 %all-gather.5.cloned.1.call-done = bf16[8,96,2048]{2,1,0:T(8,128)(2,1)} async-done(((bf16[8,96,512]{2,1,0:T(8,128)(2,1)}), bf16[8,96,2048]{2,1,0:T(8,128)(2,1)}) %all-gather.5.cloned.1.call-update) | async-done | bytes 3145744 | tf_op jit(solution)/shard_map/all_gather | solution.py:111
  121.2 6.1 %select_convert_fusion = (bf16[768,512]{1,0:T(8,128)(2,1)S(1)}, bf16[768,512]{1,0:T(8,128)(2,1)S(1)}) fusion(f32[768,512]{1,0:T(8,128)} %fusion.1, f32[768,512]{1,0:T(8,128)} %fusion.7, bf16[768,2048]{1,0:T(8,128)(2,1)} %bitcast.74, bf16[1,512,2048]{2,1,0:T(8,128)(2,1)} %param.23), kind=kOutput, calls=%fused_computation.21 | convolution fusion | flops 1619263488 | bytes 9961472 | tf_op jit(solution)/shard_map/dot_general | solution.py:34
  127.4 1.8 fusion.5
  129.6 1.8 add_convert_fusion
  131.7 39.4 %all_to_all.22 = bf16[768,4,512]{2,0,1:T(8,128)(2,1)S(1)} all-to-all(bf16[768,4,512]{2,0,1:T(8,128)(2,1)S(1)} %bitcast.55), channel_id=1, replica_groups=mesh['sp'=8,'tp'=4] {'tp'}, dimensions={1} | all-to-all | bytes 6291456 | tf_op jit(solution)/shard_map/all_to_all | solution.py:121
  171.1 1.6 convert_reduce_fusion
  172.8 5.6 %all-to-all-start.3 = ((f32[8,96,512]{2,1,0:T(8,128)}), f32[8,96,512]{2,1,0:T(8,128)S(1)}, u32[]{:S(2)}, u32[]{:S(2)}) async-start(f32[8,96,512]{2,1,0:T(8,128)} %bitcast.57), calls=%async_computation.3 | async-start | bytes 3145728 | tf_op jit(solution)/shard_map/all_to_all | solution.py:123
  178.5 36.5 %all-to-all-done.3 = f32[8,96,512]{2,1,0:T(8,128)S(1)} async-done(((f32[8,96,512]{2,1,0:T(8,128)}), f32[8,96,512]{2,1,0:T(8,128)S(1)}, u32[]{:S(2)}, u32[]{:S(2)}) %all-to-all-start.3) | async-done | bytes 1572896 | tf_op jit(solution)/shard_map/all_to_all | solution.py:123
  215.1 1.6 gather_fusion.2
  219.8 7.9 %all_gather.11 = bf16[192,2048]{1,0:T(8,128)(2,1)S(1)} all-gather(bf16[192,512]{1,0:T(8,128)(2,1)S(1)} %add_convert_fusion.1), channel_id=1, replica_groups=mesh['sp'=8,'tp'=4] {'tp'}, dimensions={1}, use_global_device_ids=true | all-gather | bytes 983040 | tf_op jit(solution)/shard_map/all_gather | solution.py:128
  228.8 3.3 %collective-permute-start = (f32[1,512]{1,0:T(1,128)S(1)}, f32[1,512]{1,0:T(1,128)S(1)}, u32[]{:S(2)}, u32[]{:S(2)}) collective-permute-start(f32[1,512]{1,0:T(1,128)S(1)} %get-tuple-element.12), channel_id=1, source_target_pairs={{0,4},{4,8},{8,12},{12,16},{16,20},{20,24},{24,28},{1,5},{5,9},{9,... | collective-permute-start | bytes 6152 | tf_op jit(solution)/shard_map/ppermute | solution.py:18
  232.1 1.5 collective-permute-start.1
  234.5 3.1 collective-permute-done.1
  237.6 1.9 fusion.21
  239.5 5.9 %convolution_bitcast_fusion.1 = f32[1,2048,512]{2,1,0:T(8,128)} fusion(bf16[768,2048]{1,0:T(8,128)(2,1)} %bitcast.71, bf16[768,512]{1,0:T(8,128)(2,1)S(1)} %copy-done.8), kind=kOutput, calls=%fused_computation.7 | convolution fusion | flops 1610612736 | bytes 8126464 | tf_op jit(solution)/shard_map/dot_general | solution.py:28
  245.4 3.9 %convolution_bitcast_fusion.2 = f32[1,2048,512]{2,1,0:T(8,128)} fusion(bf16[768,2048]{1,0:T(8,128)(2,1)S(1)} %bitcast.73, bf16[768,512]{1,0:T(8,128)(2,1)S(1)} %copy-done.6), kind=kOutput, calls=%fused_computation.8 | convolution fusion | flops 1610612736 | bytes 8126464 | tf_op jit(solution)/shard_map/dot_general | solution.py:28
  249.4 4.1 %convolution_bitcast_fusion = f32[1,512,2048]{2,1,0:T(8,128)} fusion(bf16[768,2048]{1,0:T(8,128)(2,1)S(1)} %bitcast.75, f32[768,512]{1,0:T(8,128)S(1)} %copy-done.20, f32[768,512]{1,0:T(8,128)S(1)} %copy-done.21), kind=kOutput, calls=%fused_computation.6 | convolution fusion | flops 1614544896 | bytes 10485760 | tf_op jit(solution)/shard_map/dot_general | solution.py:28
  255.0 52.5 %reduce-scatter.2.cloned.1.call-done = f32[256,256]{1,0:T(8,128)} async-done(((f32[2048,256]{1,0:T(8,128)}), f32[256,256]{1,0:T(8,128)}) %reduce-scatter.2.cloned.1.call-update) | async-done | bytes 262160 | tf_op jit(solution)/shard_map/reduce_scatter | solution.py:146
  (80 shorter events, 11.1 us)
Async XLA Ops:
  7.2 92.0 %copy-start = (bf16[1,2048,512]{2,1,0:T(8,128)(2,1)S(1)}, bf16[1,2048,512]{2,1,0:T(8,128)(2,1)}, u32[]{:S(2)}) copy-start(bf16[1,2048,512]{2,1,0:T(8,128)(2,1)} %param.21) | copy-start | bytes 6291460
  7.2 86.3 %all-gather.3.cloned.1.call-start = ((), (), s32[]{:S(2)}) async-start(), calls=%async_computation.5 | async-start | bytes 3932160 | tf_op jit(solution)/shard_map/all_gather | solution.py:110
  19.1 28.7 %copy-start.3 = (bf16[192,2048]{1,0:T(8,128)(2,1)S(1)}, bf16[192,2048]{1,0:T(8,128)(2,1)}, u32[]{:S(2)}) copy-start(bf16[192,2048]{1,0:T(8,128)(2,1)} %param.13) | copy-start | bytes 2359300
  47.7 73.6 %all-gather.5.cloned.1.call-start = ((), (), s32[]{:S(2)}) async-start(), calls=%async_computation.6 | async-start | bytes 3932160 | tf_op jit(solution)/shard_map/all_gather | solution.py:111
  51.0 5.4 %copy-start.16 = (f32[192,2]{0,1:T(2,128)S(1)}, f32[192,2]{0,1:T(2,128)}, u32[]{:S(2)}) copy-start(f32[192,2]{0,1:T(2,128)} %param.15) | copy-start | bytes 4612
  93.5 5.6 %copy-start.17 = (bf16[8,96,2048]{2,1,0:T(8,128)(2,1)S(1)}, bf16[8,96,2048]{2,1,0:T(8,128)(2,1)}, u32[]{:S(2)}) copy-start(bf16[8,96,2048]{2,1,0:T(8,128)(2,1)} %all-gather.3.cloned.1.call-done) | copy-start | bytes 9437188
  127.4 1.9 copy-start.5
  127.4 1.9 copy-start.7
  127.4 2.2 copy-start.2
  172.8 5.7 %copy-start.12 = (bf16[192,256]{1,0:T(8,128)(2,1)S(1)}, bf16[192,256]{1,0:T(8,128)(2,1)}, u32[]{:S(2)}) copy-start(bf16[192,256]{1,0:T(8,128)(2,1)} %param.18) | copy-start | bytes 294916
  172.8 5.7 %copy-start.14 = (bf16[192,256]{1,0:T(8,128)(2,1)S(1)}, bf16[192,256]{1,0:T(8,128)(2,1)}, u32[]{:S(2)}) copy-start(bf16[192,256]{1,0:T(8,128)(2,1)} %param.17) | copy-start | bytes 294916
  172.8 42.3 %all-to-all-start.3 = ((f32[8,96,512]{2,1,0:T(8,128)}), f32[8,96,512]{2,1,0:T(8,128)S(1)}, u32[]{:S(2)}, u32[]{:S(2)}) async-start(f32[8,96,512]{2,1,0:T(8,128)} %bitcast.57), calls=%async_computation.3 | async-start | bytes 3145728 | tf_op jit(solution)/shard_map/all_to_all | solution.py:123
  178.4 129.1 %reduce-scatter.2.cloned.1.call-start = ((), (), s32[]{:S(2)}) async-start(), calls=%async_computation.7 | async-start | bytes 2359296 | tf_op jit(solution)/shard_map/reduce_scatter | solution.py:146
  216.7 11.0 %copy-start.11 = (bf16[192,256]{1,0:T(8,128)(2,1)S(1)}, bf16[192,256]{1,0:T(8,128)(2,1)}, u32[]{:S(2)}) copy-start(bf16[192,256]{1,0:T(8,128)(2,1)} %param.16) | copy-start | bytes 294916
  217.2 10.5 %copy-start.4 = (bf16[2048,256]{1,0:T(8,128)(2,1)S(1)}, bf16[2048,256]{1,0:T(8,128)(2,1)}, u32[]{:S(2)}) copy-start(bf16[2048,256]{1,0:T(8,128)(2,1)} %param.20) | copy-start | bytes 3145732
  219.1 0.7 copy-start.10
  228.8 5.8 %collective-permute-start = (f32[1,512]{1,0:T(1,128)S(1)}, f32[1,512]{1,0:T(1,128)S(1)}, u32[]{:S(2)}, u32[]{:S(2)}) collective-permute-start(f32[1,512]{1,0:T(1,128)S(1)} %get-tuple-element.12), channel_id=1, source_target_pairs={{0,4},{4,8},{8,12},{12,16},{16,20},{20,24},{24,28},{1,5},{5,9},{9,... | collective-permute-start | bytes 6152 | tf_op jit(solution)/shard_map/ppermute | solution.py:18
  232.1 5.5 %collective-permute-start.1 = (f32[1,512]{1,0:T(1,128)S(1)}, f32[1,512]{1,0:T(1,128)S(1)}, u32[]{:S(2)}, u32[]{:S(2)}) collective-permute-start(f32[1,512]{1,0:T(1,128)S(1)} %get-tuple-element.13), channel_id=1, source_target_pairs={{4,0},{8,4},{12,8},{16,12},{20,16},{24,20},{28,24},{5,1},{9,5},{13... | collective-permute-start | bytes 6152 | tf_op jit(solution)/shard_map/ppermute | solution.py:20
  237.6 1.9 copy-start.8
  239.5 5.9 %copy-start.6 = (bf16[768,512]{1,0:T(8,128)(2,1)S(1)}, bf16[768,512]{1,0:T(8,128)(2,1)}, u32[]{:S(2)}) copy-start(bf16[768,512]{1,0:T(8,128)(2,1)} %copy-done.5) | copy-start | bytes 2359300
  239.5 5.9 %copy-start.18 = (bf16[8,96,2048]{2,1,0:T(8,128)(2,1)S(1)}, bf16[8,96,2048]{2,1,0:T(8,128)(2,1)}, u32[]{:S(2)}) copy-start(bf16[8,96,2048]{2,1,0:T(8,128)(2,1)} %all-gather.3.cloned.1.call-done) | copy-start | bytes 9437188
  245.4 3.9 %copy-start.19 = (bf16[8,96,2048]{2,1,0:T(8,128)(2,1)S(1)}, bf16[8,96,2048]{2,1,0:T(8,128)(2,1)}, u32[]{:S(2)}) copy-start(bf16[8,96,2048]{2,1,0:T(8,128)(2,1)} %all-gather.5.cloned.1.call-done) | copy-start | bytes 9437188
  245.4 3.9 %copy-start.20 = (f32[768,512]{1,0:T(8,128)S(1)}, f32[768,512]{1,0:T(8,128)}, u32[]{:S(2)}) copy-start(f32[768,512]{1,0:T(8,128)} %fusion.1) | copy-start | bytes 4718596
  245.4 3.9 %copy-start.21 = (f32[768,512]{1,0:T(8,128)S(1)}, f32[768,512]{1,0:T(8,128)}, u32[]{:S(2)}) copy-start(f32[768,512]{1,0:T(8,128)} %fusion.7) | copy-start | bytes 4718596
  249.4 4.1 %copy-start.13 = (bf16[192,256]{1,0:T(8,128)(2,1)S(1)}, bf16[192,256]{1,0:T(8,128)(2,1)}, u32[]{:S(2)}) copy-start(bf16[192,256]{1,0:T(8,128)(2,1)} %param.18) | copy-start | bytes 294916
  249.4 4.8 %copy-start.9 = (f32[192,256]{1,0:T(8,128)S(1)}, f32[192,256]{1,0:T(8,128)}, u32[]{:S(2)}) copy-start(f32[192,256]{1,0:T(8,128)} %get-tuple-element.20) | copy-start | bytes 589828
  249.4 4.8 %copy-start.15 = (bf16[192,256]{1,0:T(8,128)(2,1)S(1)}, bf16[192,256]{1,0:T(8,128)(2,1)}, u32[]{:S(2)}) copy-start(bf16[192,256]{1,0:T(8,128)(2,1)} %param.17) | copy-start | bytes 294916
  249.4 58.1 %copy-start.1 = (bf16[1,2048,512]{2,1,0:T(8,128)(2,1)S(1)}, bf16[1,2048,512]{2,1,0:T(8,128)(2,1)}, u32[]{:S(2)}) copy-start(bf16[1,2048,512]{2,1,0:T(8,128)(2,1)} %param.21) | copy-start | bytes 6291460
Sparse Core Ops, SparseCore 0:
  47.8 27.5 all-gather.2
  93.6 27.6 all-gather.4
  239.6 67.8 reduce-scatter.1
where the time goes:
time: 315 us; the launch traced here: 314 us
  waiting for transfers between devices  111 us (35%)
  blocking collectives  98.1 us (31%)
  local copies, waits for them, and re-layouts  35.8 us (11%)
  matrix products  35.3 us (11%)
  between operations  14.1 us (4%)
  starting transfers between devices  10.6 us (3%)
  other arithmetic  8.97 us (3%)
    reduce_scatter x1, waiting for transfers between devices, local(): lax.psum_scatter(contract_rows(residual, mixed_act), 'sp', scatter_dimens...  52.5 us
    all_to_all x1, blocking collectives, local(): lax.all_to_all(grouped, 'tp', split_axis=1, concat_axis=1, tiled=True)  39.4 us
    all_to_all x1, waiting for transfers between devices, local(): lax.all_to_all(shares, 'sp', split_axis=0, concat_axis=0, tiled=True)  36.5 us
    all_to_all x1, blocking collectives, local(): lax.all_to_all(sliced[0], 'sp', split_axis=0, concat_axis=0, tiled=True)  27.3 us
    all_to_all x1, blocking collectives, local(): lax.all_to_all(sliced[1], 'sp', split_axis=0, concat_axis=0, tiled=True)  23.4 us
    all_gather x1, waiting for transfers between devices, local(): lax.all_gather(arrived[1], 'tp', axis=2, tiled=True)  19.1 us
    dot_general x4, matrix products, contract_rows(): lax.dot_general(left, right, (((0,), (0,)), ((), ())), preferred_element_...  15.8 us
    dot_general x3, matrix products, contract_cols(): lax.dot_general(left, right, (((1,), (1,)), ((), ())), preferred_element_...  9.8 us
  transfers between devices with their start and end apart: 6, of which 4 were waited for; matrix products, arithmetic and copies ran while one was open for 15% of the time, Pallas kernels for 0%

commit v1 on v0

--- a/solution.py
+++ b/solution.py
@@ -118,7 +118,9 @@
         down_proj[0],
     )
     grouped = partial_value.reshape(expert_count * capacity, tp_count, part_width)
-    pieces = lax.all_to_all(grouped, "tp", split_axis=1, concat_axis=1, tiled=True)
+    shards = jnp.split(grouped, lax.axis_size("tp"), axis=1)
+    received = lax.all_to_all(jnp.stack(shards), "tp", 0, 0)
+    pieces = jnp.concatenate(received, axis=1)
     shares = jnp.sum(pieces.astype(jnp.float32), axis=1).reshape(expert_count, capacity, part_width)
     returned = lax.all_to_all(shares, "sp", split_axis=0, concat_axis=0, tiled=True)
     picked = returned.reshape(-1, part_width)[slot_index]

time: 315 us -> 334 us (1.060)
  local copies, waits for them, and re-layouts: 35.8 us -> 53.1 us
    split x0 -> x1, local copies, waits for them, and re-layouts: none -> 10.7 us  [local(): shards = jnp.split(grouped, lax.axis_size('tp'), axis=1)]
    reshape x1, local copies, waits for them, and re-layouts: 0.29 us -> 6.15 us  [local(): partial_value.reshape(expert_count * capacity, tp_count, part_width)]
  transfers between devices with their start and end apart: 6 -> 6, of which waited for: 4 -> 4; matrix products, arithmetic and copies ran while one was open for 15% -> 14% of each run, Pallas kernels for 0% -> 0%
where the time goes in v1:
time: 334 us
  waiting for transfers between devices  111 us (33%)
  blocking collectives  98.1 us (29%)
  local copies, waits for them, and re-layouts  53.1 us (16%)
  matrix products  36.9 us (11%)
  between operations  14.2 us (4%)
  starting transfers between devices  10.4 us (3%)
  other arithmetic  9.41 us (3%)
    reduce_scatter x1, waiting for transfers between devices, local(): lax.psum_scatter(contract_rows(residual, mixed_act), 'sp', scatter_dimens...  52.5 us
    all_to_all x1, blocking collectives, local(): received = lax.all_to_all(jnp.stack(shards), 'tp', 0, 0)  39.4 us
    all_to_all x1, waiting for transfers between devices, local(): lax.all_to_all(shares, 'sp', split_axis=0, concat_axis=0, tiled=True)  36.5 us
    all_to_all x1, blocking collectives, local(): lax.all_to_all(sliced[0], 'sp', split_axis=0, concat_axis=0, tiled=True)  27.3 us
    all_to_all x1, blocking collectives, local(): lax.all_to_all(sliced[1], 'sp', split_axis=0, concat_axis=0, tiled=True)  23.4 us
    all_gather x1, waiting for transfers between devices, local(): lax.all_gather(arrived[1], 'tp', axis=2, tiled=True)  19.1 us
    dot_general x4, matrix products, contract_rows(): lax.dot_general(left, right, (((0,), (0,)), ((), ())), preferred_element_...  15.8 us
    dot_general x3, matrix products, contract_cols(): lax.dot_general(left, right, (((1,), (1,)), ((), ())), preferred_element_...  11.5 us
  transfers between devices with their start and end apart: 6, of which 4 were waited for; matrix products, arithmetic and copies ran while one was open for 14% of the time, Pallas kernels for 0%

profile of v1, /device:TPU:0, one launch (start us, length us, event | category | flops | bytes accessed | tf_op | source)
XLA Modules:
  0.0 333.6 jit_solution(2592326290990164199)
XLA Ops:
  10.7 2.9 scatter_custom_fusion
  14.8 4.2 %gather_fusion = bf16[768,2048]{1,0:T(8,128)(2,1)} fusion(bf16[193,2048]{1,0:T(8,128)(2,1)S(1)} %concatenate.18, s32[1024]{0:T(1024)S(1)} %get-tuple-element.26), kind=kCustom, calls=%fused_computation | custom fusion | bytes 6294528 | tf_op jit(solution)/shard_map/gather | solution.py:94
  19.1 1.3 constant_dynamic-slice_fusion.2
  20.3 27.3 %all_to_all.20 = bf16[8,96,512]{2,1,0:T(8,128)(2,1)} all-to-all(bf16[8,96,512]{2,1,0:T(8,128)(2,1)S(1)} %constant_dynamic-slice_fusion.2), channel_id=1, replica_groups=mesh['sp'=8,'tp'=4] {'sp'}, dimensions={0} | all-to-all | bytes 1572864 | tf_op jit(solution)/shard_map/all_to_all | solution.py:106
  47.7 3.3 mul.141
  51.0 5.4 %mul.142 = f32[384,2048]{1,0:T(8,128)} reshape(f32[192,2,2048]{2,1,0:T(2,128)} %mul.141) | data formatting | bytes 6291456 | tf_op jit(solution)/shard_map/mul | solution.py:95
  56.7 2.1 multiply_convert_fusion
  58.8 1.3 concatenate.19
  60.1 8.7 %gather_fusion.1 = bf16[768,2048]{1,0:T(8,128)(2,1)} fusion(bf16[385,2048]{1,0:T(8,128)(2,1)} %concatenate.19, s32[1024]{0:T(1024)S(1)} %get-tuple-element.25), kind=kCustom, calls=%fused_computation.1 | custom fusion | bytes 6294528 | tf_op jit(solution)/shard_map/gather | solution.py:98
  70.0 23.4 %all_to_all.21 = bf16[8,96,512]{2,1,0:T(8,128)(2,1)} all-to-all(bf16[8,96,512]{2,1,0:T(8,128)(2,1)S(1)} %constant_dynamic-slice_fusion.1), channel_id=1, replica_groups=mesh['sp'=8,'tp'=4] {'sp'}, dimensions={0} | all-to-all | bytes 1572864 | tf_op jit(solution)/shard_map/all_to_all | solution.py:107
  93.5 5.7 %fusion.1 = f32[768,512]{1,0:T(8,128)} fusion(bf16[768,2048]{1,0:T(8,128)(2,1)} %bitcast.80, bf16[1,2048,512]{2,1,0:T(8,128)(2,1)} %param.22), kind=kOutput, calls=%fused_computation.12 | convolution fusion | flops 1610612736 | bytes 6815744 | tf_op jit(solution)/shard_map/dot_general | solution.py:41
  99.2 3.0 fusion.7
  102.2 19.1 %all-gather.5.cloned.1.call-done = bf16[8,96,2048]{2,1,0:T(8,128)(2,1)} async-done(((bf16[8,96,512]{2,1,0:T(8,128)(2,1)}), bf16[8,96,2048]{2,1,0:T(8,128)(2,1)}) %all-gather.5.cloned.1.call-update) | async-done | bytes 3145744 | tf_op jit(solution)/shard_map/all_gather | solution.py:111
  121.2 6.1 %select_convert_fusion = (bf16[768,512]{1,0:T(8,128)(2,1)S(1)}, bf16[768,512]{1,0:T(8,128)(2,1)S(1)}) fusion(f32[768,512]{1,0:T(8,128)} %fusion.1, f32[768,512]{1,0:T(8,128)} %fusion.7, bf16[768,2048]{1,0:T(8,128)(2,1)} %bitcast.84, bf16[1,512,2048]{2,1,0:T(8,128)(2,1)} %param.23), kind=kOutput, calls=%fused_computation.21 | convolution fusion | flops 1619263488 | bytes 9961472 | tf_op jit(solution)/shard_map/dot_general | solution.py:34
  127.4 1.8 fusion.5
  129.6 3.5 %add_convert_fusion = bf16[768,2048]{1,0:T(8,128)(2,1)} fusion(f32[768,2048]{1,0:T(8,128)S(1)} %fusion.5, bf16[768,512]{1,0:T(8,128)(2,1)S(1)} %get-tuple-element.8, bf16[1,2048,512]{2,1,0:T(8,128)(2,1)S(1)} %copy-done.2), kind=kOutput, calls=%fused_computation.5 | convolution fusion | flops 1613758464 | bytes 12320768 | tf_op jit(solution)/shard_map/dot_general | solution.py:34
  133.1 6.1 %reshape.102 = bf16[768,4,512]{2,1,0:T(4,128)(2,1)} reshape(bf16[768,2048]{1,0:T(8,128)(2,1)} %add_convert_fusion) | data formatting | bytes 6291456 | tf_op jit(solution)/shard_map/reshape | solution.py:120
  139.2 10.7 %fusion.34 = (bf16[768,1,512]{2,1,0:T(2,128)(2,1)S(1)}, bf16[768,1,512]{2,1,0:T(2,128)(2,1)S(1)}, bf16[768,1,512]{2,1,0:T(2,128)(2,1)S(1)}, bf16[768,1,512]{2,1,0:T(2,128)(2,1)S(1)}) fusion(bf16[768,4,512]{2,1,0:T(4,128)(2,1)} %reshape.102), kind=kLoop, calls=%fused_computation.88 | loop fusion | bytes 6291456 | tf_op jit(solution)/shard_map/split | solution.py:121
  151.2 39.4 %all_to_all.22 = bf16[4,768,1,512]{3,1,2,0:T(8,128)(2,1)S(1)} all-to-all(bf16[4,768,1,512]{3,1,2,0:T(8,128)(2,1)S(1)} %pad_maximum_fusion), channel_id=1, replica_groups=mesh['sp'=8,'tp'=4] {'tp'}, dimensions={0} | all-to-all | bytes 6291456 | tf_op jit(solution)/shard_map/all_to_all | solution.py:122
  190.6 1.6 convert_reduce_fusion
  192.3 5.6 %all-to-all-start.3 = ((f32[8,96,512]{2,1,0:T(8,128)}), f32[8,96,512]{2,1,0:T(8,128)S(1)}, u32[]{:S(2)}, u32[]{:S(2)}) async-start(f32[8,96,512]{2,1,0:T(8,128)} %bitcast.63), calls=%async_computation.3 | async-start | bytes 3145728 | tf_op jit(solution)/shard_map/all_to_all | solution.py:125
  198.0 36.5 %all-to-all-done.3 = f32[8,96,512]{2,1,0:T(8,128)S(1)} async-done(((f32[8,96,512]{2,1,0:T(8,128)}), f32[8,96,512]{2,1,0:T(8,128)S(1)}, u32[]{:S(2)}, u32[]{:S(2)}) %all-to-all-start.3) | async-done | bytes 1572896 | tf_op jit(solution)/shard_map/all_to_all | solution.py:125
  234.6 1.6 gather_fusion.2
  239.3 7.9 %all_gather.11 = bf16[192,2048]{1,0:T(8,128)(2,1)S(1)} all-gather(bf16[192,512]{1,0:T(8,128)(2,1)S(1)} %add_convert_fusion.1), channel_id=1, replica_groups=mesh['sp'=8,'tp'=4] {'tp'}, dimensions={1}, use_global_device_ids=true | all-gather | bytes 983040 | tf_op jit(solution)/shard_map/all_gather | solution.py:130
  248.2 3.3 %collective-permute-start = (f32[1,512]{1,0:T(1,128)S(1)}, f32[1,512]{1,0:T(1,128)S(1)}, u32[]{:S(2)}, u32[]{:S(2)}) collective-permute-start(f32[1,512]{1,0:T(1,128)S(1)} %get-tuple-element.16), channel_id=1, source_target_pairs={{0,4},{4,8},{8,12},{12,16},{16,20},{20,24},{24,28},{1,5},{5,9},{9,... | collective-permute-start | bytes 6152 | tf_op jit(solution)/shard_map/ppermute | solution.py:18
  251.6 1.3 collective-permute-start.1
  253.8 3.3 collective-permute-done.1
  257.1 1.9 fusion.21
  259.0 5.9 %convolution_bitcast_fusion.1 = f32[1,2048,512]{2,1,0:T(8,128)} fusion(bf16[768,2048]{1,0:T(8,128)(2,1)} %bitcast.81, bf16[768,512]{1,0:T(8,128)(2,1)S(1)} %copy-done.8), kind=kOutput, calls=%fused_computation.7 | convolution fusion | flops 1610612736 | bytes 8126464 | tf_op jit(solution)/shard_map/dot_general | solution.py:28
  264.9 3.9 %convolution_bitcast_fusion.2 = f32[1,2048,512]{2,1,0:T(8,128)} fusion(bf16[768,2048]{1,0:T(8,128)(2,1)S(1)} %bitcast.83, bf16[768,512]{1,0:T(8,128)(2,1)S(1)} %copy-done.6), kind=kOutput, calls=%fused_computation.8 | convolution fusion | flops 1610612736 | bytes 8126464 | tf_op jit(solution)/shard_map/dot_general | solution.py:28
  268.9 4.1 %convolution_bitcast_fusion = f32[1,512,2048]{2,1,0:T(8,128)} fusion(bf16[768,2048]{1,0:T(8,128)(2,1)S(1)} %bitcast.85, f32[768,512]{1,0:T(8,128)S(1)} %copy-done.20, f32[768,512]{1,0:T(8,128)S(1)} %copy-done.21), kind=kOutput, calls=%fused_computation.6 | convolution fusion | flops 1614544896 | bytes 10485760 | tf_op jit(solution)/shard_map/dot_general | solution.py:28
  274.5 52.5 %reduce-scatter.2.cloned.1.call-done = f32[256,256]{1,0:T(8,128)} async-done(((f32[2048,256]{1,0:T(8,128)}), f32[256,256]{1,0:T(8,128)}) %reduce-scatter.2.cloned.1.call-update) | async-done | bytes 262160 | tf_op jit(solution)/shard_map/reduce_scatter | solution.py:148
  (86 shorter events, 14.5 us)
Async XLA Ops:
  7.2 92.0 %copy-start = (bf16[1,2048,512]{2,1,0:T(8,128)(2,1)S(1)}, bf16[1,2048,512]{2,1,0:T(8,128)(2,1)}, u32[]{:S(2)}) copy-start(bf16[1,2048,512]{2,1,0:T(8,128)(2,1)} %param.21) | copy-start | bytes 6291460
  7.2 86.3 %all-gather.3.cloned.1.call-start = ((), (), s32[]{:S(2)}) async-start(), calls=%async_computation.5 | async-start | bytes 3932160 | tf_op jit(solution)/shard_map/all_gather | solution.py:110
  19.1 28.7 %copy-start.3 = (bf16[192,2048]{1,0:T(8,128)(2,1)S(1)}, bf16[192,2048]{1,0:T(8,128)(2,1)}, u32[]{:S(2)}) copy-start(bf16[192,2048]{1,0:T(8,128)(2,1)} %param.13) | copy-start | bytes 2359300
  47.7 73.6 %all-gather.5.cloned.1.call-start = ((), (), s32[]{:S(2)}) async-start(), calls=%async_computation.6 | async-start | bytes 3932160 | tf_op jit(solution)/shard_map/all_gather | solution.py:111
  51.0 5.4 %copy-start.16 = (f32[192,2]{0,1:T(2,128)S(1)}, f32[192,2]{0,1:T(2,128)}, u32[]{:S(2)}) copy-start(f32[192,2]{0,1:T(2,128)} %param.15) | copy-start | bytes 4612
  93.5 5.7 %copy-start.17 = (bf16[8,96,2048]{2,1,0:T(8,128)(2,1)S(1)}, bf16[8,96,2048]{2,1,0:T(8,128)(2,1)}, u32[]{:S(2)}) copy-start(bf16[8,96,2048]{2,1,0:T(8,128)(2,1)} %all-gather.3.cloned.1.call-done) | copy-start | bytes 9437188
  127.4 1.9 copy-start.5
  127.4 1.9 copy-start.7
  127.4 2.2 copy-start.2
  192.3 5.7 %copy-start.12 = (bf16[192,256]{1,0:T(8,128)(2,1)S(1)}, bf16[192,256]{1,0:T(8,128)(2,1)}, u32[]{:S(2)}) copy-start(bf16[192,256]{1,0:T(8,128)(2,1)} %param.18) | copy-start | bytes 294916
  192.3 5.7 %copy-start.14 = (bf16[192,256]{1,0:T(8,128)(2,1)S(1)}, bf16[192,256]{1,0:T(8,128)(2,1)}, u32[]{:S(2)}) copy-start(bf16[192,256]{1,0:T(8,128)(2,1)} %param.17) | copy-start | bytes 294916
  192.3 42.3 %all-to-all-start.3 = ((f32[8,96,512]{2,1,0:T(8,128)}), f32[8,96,512]{2,1,0:T(8,128)S(1)}, u32[]{:S(2)}, u32[]{:S(2)}) async-start(f32[8,96,512]{2,1,0:T(8,128)} %bitcast.63), calls=%async_computation.3 | async-start | bytes 3145728 | tf_op jit(solution)/shard_map/all_to_all | solution.py:125
  197.9 129.1 %reduce-scatter.2.cloned.1.call-start = ((), (), s32[]{:S(2)}) async-start(), calls=%async_computation.7 | async-start | bytes 2359296 | tf_op jit(solution)/shard_map/reduce_scatter | solution.py:148
  236.2 11.0 %copy-start.11 = (bf16[192,256]{1,0:T(8,128)(2,1)S(1)}, bf16[192,256]{1,0:T(8,128)(2,1)}, u32[]{:S(2)}) copy-start(bf16[192,256]{1,0:T(8,128)(2,1)} %param.16) | copy-start | bytes 294916
  236.7 10.5 %copy-start.4 = (bf16[2048,256]{1,0:T(8,128)(2,1)S(1)}, bf16[2048,256]{1,0:T(8,128)(2,1)}, u32[]{:S(2)}) copy-start(bf16[2048,256]{1,0:T(8,128)(2,1)} %param.20) | copy-start | bytes 3145732
  238.6 0.7 copy-start.10
  248.2 5.5 %collective-permute-start = (f32[1,512]{1,0:T(1,128)S(1)}, f32[1,512]{1,0:T(1,128)S(1)}, u32[]{:S(2)}, u32[]{:S(2)}) collective-permute-start(f32[1,512]{1,0:T(1,128)S(1)} %get-tuple-element.16), channel_id=1, source_target_pairs={{0,4},{4,8},{8,12},{12,16},{16,20},{20,24},{24,28},{1,5},{5,9},{9,... | collective-permute-start | bytes 6152 | tf_op jit(solution)/shard_map/ppermute | solution.py:18
  251.6 5.5 %collective-permute-start.1 = (f32[1,512]{1,0:T(1,128)S(1)}, f32[1,512]{1,0:T(1,128)S(1)}, u32[]{:S(2)}, u32[]{:S(2)}) collective-permute-start(f32[1,512]{1,0:T(1,128)S(1)} %get-tuple-element.17), channel_id=1, source_target_pairs={{4,0},{8,4},{12,8},{16,12},{20,16},{24,20},{28,24},{5,1},{9,5},{13... | collective-permute-start | bytes 6152 | tf_op jit(solution)/shard_map/ppermute | solution.py:20
  257.1 1.9 copy-start.8
  259.0 5.9 %copy-start.6 = (bf16[768,512]{1,0:T(8,128)(2,1)S(1)}, bf16[768,512]{1,0:T(8,128)(2,1)}, u32[]{:S(2)}) copy-start(bf16[768,512]{1,0:T(8,128)(2,1)} %copy-done.5) | copy-start | bytes 2359300
  259.0 5.9 %copy-start.18 = (bf16[8,96,2048]{2,1,0:T(8,128)(2,1)S(1)}, bf16[8,96,2048]{2,1,0:T(8,128)(2,1)}, u32[]{:S(2)}) copy-start(bf16[8,96,2048]{2,1,0:T(8,128)(2,1)} %all-gather.3.cloned.1.call-done) | copy-start | bytes 9437188
  264.9 3.9 %copy-start.19 = (bf16[8,96,2048]{2,1,0:T(8,128)(2,1)S(1)}, bf16[8,96,2048]{2,1,0:T(8,128)(2,1)}, u32[]{:S(2)}) copy-start(bf16[8,96,2048]{2,1,0:T(8,128)(2,1)} %all-gather.5.cloned.1.call-done) | copy-start | bytes 9437188
  264.9 3.9 %copy-start.20 = (f32[768,512]{1,0:T(8,128)S(1)}, f32[768,512]{1,0:T(8,128)}, u32[]{:S(2)}) copy-start(f32[768,512]{1,0:T(8,128)} %fusion.1) | copy-start | bytes 4718596
  264.9 3.9 %copy-start.21 = (f32[768,512]{1,0:T(8,128)S(1)}, f32[768,512]{1,0:T(8,128)}, u32[]{:S(2)}) copy-start(f32[768,512]{1,0:T(8,128)} %fusion.7) | copy-start | bytes 4718596
  268.9 4.1 %copy-start.13 = (bf16[192,256]{1,0:T(8,128)(2,1)S(1)}, bf16[192,256]{1,0:T(8,128)(2,1)}, u32[]{:S(2)}) copy-start(bf16[192,256]{1,0:T(8,128)(2,1)} %param.18) | copy-start | bytes 294916
  268.9 4.8 %copy-start.9 = (f32[192,256]{1,0:T(8,128)S(1)}, f32[192,256]{1,0:T(8,128)}, u32[]{:S(2)}) copy-start(f32[192,256]{1,0:T(8,128)} %get-tuple-element.24) | copy-start | bytes 589828
  268.9 4.8 %copy-start.15 = (bf16[192,256]{1,0:T(8,128)(2,1)S(1)}, bf16[192,256]{1,0:T(8,128)(2,1)}, u32[]{:S(2)}) copy-start(bf16[192,256]{1,0:T(8,128)(2,1)} %param.17) | copy-start | bytes 294916
  268.9 58.2 %copy-start.1 = (bf16[1,2048,512]{2,1,0:T(8,128)(2,1)S(1)}, bf16[1,2048,512]{2,1,0:T(8,128)(2,1)}, u32[]{:S(2)}) copy-start(bf16[1,2048,512]{2,1,0:T(8,128)(2,1)} %param.21) | copy-start | bytes 6291460
Sparse Core Ops, SparseCore 0:
  47.8 27.5 all-gather.2
  93.6 27.6 all-gather.4
  259.1 67.8 reduce-scatter.1
